TPU v7x, 256 devices: a whole 4x4x8 slice. The times are simulated.
256 devices in a mesh: sp: 64 (over z, y, core), tp: 4 (over x).
Axes of the slice: x: 4, y: 4, z: 8, core: 2. Of those that a mesh axis runs over, the one named last changes fastest.
Arguments:
- stream: bfloat16 [32768, 2048], P(('sp', 'tp')), may hold values from -6 to 6
- conv_value: bfloat16 [32768, 512], P('sp', 'tp'), may hold values from -6 to 6
- conv_gate: bfloat16 [32768, 512], P('sp', 'tp'), may hold values from -8 to 8
- doc_ids: int32 [32768], P('sp'), may hold values from 0 to 31, never falling along the last dimension, each value on 1 to 2048 neighbouring positions
- conv_taps: float32 [31, 512], P(None, 'tp'), may hold values from -2.2 to 2.2
- conv_bias: float32 [512], P('tp'), may hold values from -3 to 3
- chan_gain: float32 [512], replicated, may hold values from 0.1 to 1.9
- chan_shift: float32 [512], replicated, may hold values from -3 to 3
- out_weight: bfloat16 [512, 2048], replicated, may hold values from -0.25 to 0.25
- rms_gain: float32 [2048], replicated, may hold values from 0.1 to 1.9
- expert_ids: int32 [32768, 2], P(('sp', 'tp')), may hold values from 0 to 127, all different within a row; in each aligned block of 128 rows (0 to 127, 128 to 255, ...) at most 3 rows name the same one
- group_prob: float32 [32768], P(('sp', 'tp')), may hold values from 0.3 to 1
- route_logits: float32 [32768, 2], P(('sp', 'tp')), may hold values from -6 to 6
- expert_gate: bfloat16 [128, 2048, 1024], P('sp', None, 'tp'), may hold values from -0.125 to 0.125
- expert_up: bfloat16 [128, 2048, 1024], P('sp', None, 'tp'), may hold values from -0.125 to 0.125
- expert_down: bfloat16 [128, 1024, 2048], P('sp', 'tp'), may hold values from -0.1875 to 0.1875
Outputs:
- mixed: bfloat16 [32768, 2048], P(('sp', 'tp'))
Inputs may be any that keep to these rules, and one draw needn't show every extreme that they name: `expert_ids`: each row names 2 different experts. In each aligned block of 128 rows (the rows of one device) no expert is named by more than 3 rows, a bound that some block reaches. `doc_ids`: document numbers never fall along the sequence; every document has 1 to 2048 positions, one exactly 2048.
All inputs are finite; a program needn't handle non-finite values.
Results may differ from a plain program's by a relative error of at most 0.012.
Values may be sent and summed in bfloat16 or wider, within the bound.
A program may use at most 64 MiB of HBM per device.

v0:
```python
import jax
import jax.numpy as jnp
from jax import lax
from jax.sharding import PartitionSpec as P

eps = 1e-06


def passed_along(x, axis, by):
    size = lax.axis_size(axis)
    pairs = [(i, i + by) for i in range(size) if 0 <= i + by < size]
    return lax.ppermute(x, axis, pairs)


def causal_conv(values, gates, docs, conv_taps, conv_bias):
    reach = conv_taps.shape[0] - 1
    acts = values.astype(jnp.float32) * jax.nn.sigmoid(gates.astype(jnp.float32))
    total = values.shape[0] - reach
    result = jnp.broadcast_to(conv_bias[None, :], (total, values.shape[1]))
    own_doc = docs[reach:]
    for offset in range(reach + 1):
        begin = reach - offset
        same = (docs[begin : begin + total] == own_doc)[:, None]
        result = (
            result + jnp.where(same, acts[begin : begin + total], 0.0) * conv_taps[offset][None, :]
        )
    return result.astype(jnp.bfloat16)


def finish_norm(values, mean, square, gain, shift):
    spread = square - mean * mean
    scaled = (values - mean) * lax.rsqrt(spread + eps) * gain + shift
    return jax.nn.silu(scaled).astype(jnp.bfloat16)


def apply_experts(arrived, expert_gate, expert_up, expert_down):
    outputs = []
    for local in range(arrived.shape[1]):
        rows = arrived[:, local].reshape(-1, arrived.shape[3])
        gated = jnp.dot(rows, expert_gate[local], preferred_element_type=jnp.float32)
        upward = jnp.dot(rows, expert_up[local], preferred_element_type=jnp.float32)
        hidden = (jax.nn.silu(gated) * upward).astype(jnp.bfloat16)
        partial_value = jnp.dot(hidden, expert_down[local], preferred_element_type=jnp.float32)
        outputs.append(partial_value.reshape(arrived.shape[0], arrived.shape[2], arrived.shape[3]))
    return jnp.stack(outputs, axis=1)


def split_quarters(partial_value, quarters):
    shape = partial_value.shape
    return partial_value.astype(jnp.bfloat16).reshape(
        shape[0], shape[1], quarters, shape[2] // quarters, shape[3]
    )


def body(
    stream,
    conv_value,
    conv_gate,
    doc_ids,
    conv_taps,
    conv_bias,
    chan_gain,
    chan_shift,
    out_weight,
    rms_gain,
    expert_ids,
    group_prob,
    route_logits,
    expert_gate,
    expert_up,
    expert_down,
):
    reach = conv_taps.shape[0] - 1
    tail_value, tail_gate, tail_doc = passed_along(
        (conv_value[-reach:], conv_gate[-reach:], doc_ids[-reach:]), "sp", 1
    )
    values = jnp.concatenate([tail_value, conv_value], axis=0)
    gates = jnp.concatenate([tail_gate, conv_gate], axis=0)
    docs = jnp.concatenate([tail_doc, doc_ids], axis=0)
    conved = causal_conv(values, gates, docs, conv_taps, conv_bias)
    own_rows = stream.shape[0]
    regrouped = lax.all_to_all(conved, "tp", split_axis=0, concat_axis=1, tiled=True)
    floats = regrouped.astype(jnp.float32)
    mean = jnp.mean(floats, axis=-1, keepdims=True)
    square = jnp.mean(floats * floats, axis=-1, keepdims=True)
    activated = finish_norm(floats, mean, square, chan_gain, chan_shift)
    projected = jnp.dot(activated, out_weight, preferred_element_type=jnp.float32)
    resid = (stream.astype(jnp.float32) + projected).astype(jnp.bfloat16)
    resid_float = resid.astype(jnp.float32)
    mean_square = jnp.mean(resid_float * resid_float, axis=-1, keepdims=True)
    normed = (resid_float * lax.rsqrt(mean_square + eps) * rms_gain).astype(jnp.bfloat16)
    gap = route_logits[:, 0] - route_logits[:, 1]
    weights = jnp.stack(
        [group_prob * jax.nn.sigmoid(gap), group_prob * jax.nn.sigmoid(-gap)], axis=1
    )
    sp_count = lax.axis_size("sp")
    tp_count = lax.axis_size("tp")
    local_experts = expert_gate.shape[0]
    experts_all = sp_count * local_experts
    top_count = expert_ids.shape[1]
    capacity = max(2, 3 * own_rows * top_count // (2 * experts_all))
    flat_ids = expert_ids.reshape(-1)
    onehot = (flat_ids[:, None] == jnp.arange(experts_all, dtype=jnp.int32)[None, :]).astype(
        jnp.int32
    )
    earlier = jnp.cumsum(onehot, axis=0) - onehot
    ranks = jnp.sum(earlier * onehot, axis=1)
    dest = flat_ids * capacity + ranks
    route_token = jnp.arange(flat_ids.shape[0], dtype=jnp.int32) // top_count
    source = jnp.full((experts_all * capacity,), own_rows, jnp.int32).at[dest].set(route_token)
    with_blank = jnp.concatenate([normed, jnp.zeros((1, normed.shape[1]), jnp.bfloat16)], axis=0)
    outgoing = with_blank[source].reshape(sp_count, local_experts, capacity, normed.shape[1])
    arrived_own = lax.all_to_all(outgoing, "sp", split_axis=0, concat_axis=0, tiled=True)
    arrived = lax.all_gather(arrived_own, "tp", axis=2, tiled=True)
    partial_value = apply_experts(arrived, expert_gate, expert_up, expert_down)
    quarters = lax.all_to_all(
        split_quarters(partial_value, tp_count), "tp", split_axis=2, concat_axis=2, tiled=True
    )
    summed = jnp.sum(quarters.astype(jnp.float32), axis=2).astype(jnp.bfloat16)
    routed = lax.all_to_all(summed, "sp", split_axis=0, concat_axis=0, tiled=True)
    flat_out = routed.reshape(experts_all * capacity, normed.shape[1])
    picked = flat_out[dest].reshape(own_rows, top_count, normed.shape[1]).astype(jnp.float32)
    combined = jnp.sum(weights[:, :, None] * picked, axis=1)
    return (resid_float + combined).astype(jnp.bfloat16)


def solution(mesh):
    placed = (
        P(("sp", "tp"), None),
        P("sp", "tp"),
        P("sp", "tp"),
        P("sp"),
        P(None, "tp"),
        P("tp"),
        P(),
        P(),
        P(),
        P(),
        P(("sp", "tp"), None),
        P(("sp", "tp")),
        P(("sp", "tp"), None),
        P("sp", None, "tp"),
        P("sp", None, "tp"),
        P("sp", "tp", None),
    )
    return jax.shard_map(
        body, mesh=mesh, in_specs=placed, out_specs=P(("sp", "tp"), None), check_vma=False
    )
```

profile of v0, /device:TPU:1, one launch (start us, length us, event | category | flops | bytes accessed | tf_op | source)
XLA Modules:
  0.0 369.9 jit_solution(13380096626957042728)
XLA Ops:
  7.5 4.6 %collective-permute-start.2 = (s32[30]{0:T(128)S(1)}, s32[30]{0:T(128)S(1)}, u32[]{:S(2)}, u32[]{:S(2)}) collective-permute-start(s32[30]{0:T(128)S(1)} %slice.325), channel_id=1, source_target_pairs={{0,4},{4,8},{8,12},{12,16},{16,20},{20,24},{24,28},{28,32},{32,36}... | collective-permute-start | bytes 368 | tf_op jit(solution)/shard_map/ppermute | solution.py:12
  12.7 1.9 collective-permute-start
  15.4 3.6 collective-permute-start.1
  28.4 3.4 fusion.25
  31.8 4.0 %all-to-all-start = ((bf16[4,128,128]{2,1,0:T(8,128)(2,1)}), bf16[4,128,128]{2,1,0:T(8,128)(2,1)S(1)}, u32[]{:S(2)}, u32[]{:S(2)}) async-start(bf16[4,128,128]{2,1,0:T(8,128)(2,1)} %bitcast.31), calls=%async_computation | async-start | bytes 262144 | tf_op jit(solution)/shard_map/all_to_all | solution.py:82
  35.9 5.1 %all-to-all-done = bf16[4,128,128]{2,1,0:T(8,128)(2,1)S(1)} async-done(((bf16[4,128,128]{2,1,0:T(8,128)(2,1)}), bf16[4,128,128]{2,1,0:T(8,128)(2,1)S(1)}, u32[]{:S(2)}, u32[]{:S(2)}) %all-to-all-start) | async-done | bytes 131104 | tf_op jit(solution)/shard_map/all_to_all | solution.py:82
  43.3 3.1 gather_fusion
  46.5 4.0 %reshape.161 = bf16[64,2,3,2048]{3,2,1,0:T(4,128)(2,1)S(1)} reshape(bf16[384,2048]{1,0:T(8,128)(2,1)} %gather_fusion) | data formatting | bytes 3145728 | tf_op jit(solution)/shard_map/reshape | solution.py:112
  50.5 2.1 copy.44
  52.6 50.4 %all_to_all.28 = bf16[64,2,3,2048]{3,1,2,0:T(2,128)(2,1)S(1)} all-to-all(bf16[64,2,3,2048]{3,1,2,0:T(2,128)(2,1)S(1)} %copy.44), channel_id=1, replica_groups=mesh['sp'=64,'tp'=4] {'sp'}, dimensions={0} | all-to-all | bytes 3145728 | tf_op jit(solution)/shard_map/all_to_all | solution.py:113
  103.0 1.8 copy.45
  104.8 63.3 %all-gather.2.cloned.1.call-done = bf16[64,2,12,2048]{3,0,1,2:T(8,128)(2,1)} async-done(((bf16[64,2,3,2048]{3,0,1,2:T(8,128)(2,1)}), bf16[64,2,12,2048]{3,0,1,2:T(8,128)(2,1)}) %all-gather.2.cloned.1.call-update) | async-done | bytes 6291472 | tf_op jit(solution)/shard_map/all_gather | solution.py:114
  168.1 5.3 %fusion.97 = (bf16[64,1,12,2048]{3,0,1,2:T(8,128)(2,1)S(1)}, bf16[64,1,12,2048]{3,0,1,2:T(8,128)(2,1)}) fusion(bf16[64,2,12,2048]{3,0,1,2:T(8,128)(2,1)} %all-gather.2.cloned.1.call-done), kind=kLoop, calls=%fused_computation.230 | loop fusion | bytes 12582912 | tf_op jit(solution)/shard_map/slice | solution.py:39
  173.5 3.7 %copy.46 = bf16[64,1,12,2048]{3,2,0,1:T(8,128)(2,1)} copy(bf16[64,1,12,2048]{3,0,1,2:T(8,128)(2,1)S(1)} %get-tuple-element.7) | data formatting | bytes 6291456 | tf_op jit(solution)/shard_map/slice | solution.py:39
  177.2 6.3 %reshape_squeeze.6 = bf16[768,2048]{1,0:T(8,128)(2,1)} reshape(bf16[64,1,12,2048]{3,2,0,1:T(8,128)(2,1)} %copy.46) | data formatting | bytes 6291456 | tf_op jit(solution)/shard_map/reshape;squeeze | solution.py:39
  183.5 3.0 fusion.12
  189.0 5.6 %copy.48 = bf16[64,1,12,2048]{3,2,0,1:T(8,128)(2,1)} copy(bf16[64,1,12,2048]{3,0,1,2:T(8,128)(2,1)} %get-tuple-element.8) | data formatting | bytes 6291456 | tf_op jit(solution)/shard_map/slice | solution.py:39
  194.6 6.3 %reshape_squeeze.7 = bf16[768,2048]{1,0:T(8,128)(2,1)} reshape(bf16[64,1,12,2048]{3,2,0,1:T(8,128)(2,1)} %copy.48) | data formatting | bytes 6291456 | tf_op jit(solution)/shard_map/reshape;squeeze | solution.py:39
  201.0 3.0 fusion.9
  204.4 1.7 fusion.5
  206.2 2.1 reshape.163
  208.2 2.1 fusion
  213.1 73.9 %all_to_all.29 = bf16[64,2,4,3,2048]{4,0,3,1,2:T(8,128)(2,1)} all-to-all(bf16[64,2,4,3,2048]{4,0,3,1,2:T(8,128)(2,1)S(1)} %copy.50), channel_id=1, replica_groups=mesh['sp'=64,'tp'=4] {'tp'}, dimensions={2} | all-to-all | bytes 12582912 | tf_op jit(solution)/shard_map/all_to_all | solution.py:116
  287.0 4.2 %reduce_sum.64 = bf16[64,2,3,2048]{3,0,2,1:T(8,128)(2,1)S(1)} reduce(bf16[64,2,4,3,2048]{4,0,3,1,2:T(8,128)(2,1)} %all_to_all.29, bf16[]{:T(256)} %constant.46.clone.1), dimensions={2}, to_apply=%region_7.8 | reduce | flops 2359296 | bytes 7864322 | tf_op jit(solution)/shard_map/reduce_sum | solution.py:119
  291.2 2.8 copy.52
  293.9 12.1 %all-to-all-start.3 = ((bf16[64,2,3,2048]{3,1,2,0:T(2,128)(2,1)}), bf16[64,2,3,2048]{3,1,2,0:T(2,128)(2,1)S(1)}, u32[]{:S(2)}, u32[]{:S(2)}) async-start(bf16[64,2,3,2048]{3,1,2,0:T(2,128)(2,1)} %copy.52), calls=%async_computation.3 | async-start | bytes 3145728 | tf_op jit(solution)/shard_map/all_to_all | solution.py:120
  306.2 38.9 %all-to-all-done.3 = bf16[64,2,3,2048]{3,1,2,0:T(2,128)(2,1)S(1)} async-done(((bf16[64,2,3,2048]{3,1,2,0:T(2,128)(2,1)}), bf16[64,2,3,2048]{3,1,2,0:T(2,128)(2,1)S(1)}, u32[]{:S(2)}, u32[]{:S(2)}) %all-to-all-start.3) | async-done | bytes 1572896 | tf_op jit(solution)/shard_map/all_to_all | solution.py:120
  345.1 2.4 copy.53
  347.5 3.9 %reshape.164 = bf16[384,2048]{1,0:T(8,128)(2,1)S(1)} reshape(bf16[64,2,3,2048]{3,2,1,0:T(4,128)(2,1)} %copy.53) | data formatting | bytes 3145728 | tf_op jit(solution)/shard_map/reshape | solution.py:121
  351.4 2.3 gather_fusion.1
  353.8 3.4 reshape.168
  357.1 5.0 %multiply_reduce_fusion = f32[128,2048]{1,0:T(8,128)S(1)} fusion(f32[128,2,2048]{2,1,0:T(2,128)} %reshape.168, f32[128,2]{1,0:T(8,128)S(1)} %copy.38), kind=kLoop, calls=%fused_computation.11 | loop fusion | flops 786432 | bytes 3146752 | tf_op jit(solution)/shard_map/reduce_sum | solution.py:123
  (85 shorter events, 20.7 us)
Async XLA Ops:
  6.5 35.0 %copy-start = (bf16[512,2048]{1,0:T(8,128)(2,1)S(1)}, bf16[512,2048]{1,0:T(8,128)(2,1)}, u32[]{:S(2)}) copy-start(bf16[512,2048]{1,0:T(8,128)(2,1)} %param.24) | copy-start | bytes 6291460
  6.5 21.8 %copy-start.11 = (f32[128]{0:T(128)S(1)}, f32[128]{0:T(128)}, u32[]{:S(2)}) copy-start(f32[128]{0:T(128)} %param.21) | copy-start | bytes 1540
  7.5 17.5 %collective-permute-start.2 = (s32[30]{0:T(128)S(1)}, s32[30]{0:T(128)S(1)}, u32[]{:S(2)}, u32[]{:S(2)}) collective-permute-start(s32[30]{0:T(128)S(1)} %slice.325), channel_id=1, source_target_pairs={{0,4},{4,8},{8,12},{12,16},{16,20},{20,24},{24,28},{28,32},{32,36}... | collective-permute-start | bytes 368 | tf_op jit(solution)/shard_map/ppermute | solution.py:12
  12.7 14.5 %collective-permute-start = (bf16[30,128]{1,0:T(8,128)(2,1)S(1)}, bf16[30,128]{1,0:T(8,128)(2,1)S(1)}, u32[]{:S(2)}, u32[]{:S(2)}) collective-permute-start(bf16[30,128]{1,0:T(8,128)(2,1)S(1)} %slice.321), channel_id=1, source_target_pairs={{0,4},{4,8},{8,12},{12,16},{16,20},{20,24},{24,28},{28,32},{32,36}... | collective-permute-start | bytes 23048 | tf_op jit(solution)/shard_map/ppermute | solution.py:12
  15.4 11.9 %collective-permute-start.1 = (bf16[30,128]{1,0:T(8,128)(2,1)S(1)}, bf16[30,128]{1,0:T(8,128)(2,1)S(1)}, u32[]{:S(2)}, u32[]{:S(2)}) collective-permute-start(bf16[30,128]{1,0:T(8,128)(2,1)S(1)} %slice.322), channel_id=1, source_target_pairs={{0,4},{4,8},{8,12},{12,16},{16,20},{20,24},{24,28},{28,32},{32,36}... | collective-permute-start | bytes 23048 | tf_op jit(solution)/shard_map/ppermute | solution.py:12
  28.4 12.9 %copy-start.7 = (f32[512]{0:T(512)S(1)}, f32[512]{0:T(512)}, u32[]{:S(2)}) copy-start(f32[512]{0:T(512)} %param.23) | copy-start | bytes 6148
  28.4 12.9 %copy-start.8 = (f32[512]{0:T(512)S(1)}, f32[512]{0:T(512)}, u32[]{:S(2)}) copy-start(f32[512]{0:T(512)} %param.22) | copy-start | bytes 6148
  31.8 9.1 %all-to-all-start = ((bf16[4,128,128]{2,1,0:T(8,128)(2,1)}), bf16[4,128,128]{2,1,0:T(8,128)(2,1)S(1)}, u32[]{:S(2)}, u32[]{:S(2)}) async-start(bf16[4,128,128]{2,1,0:T(8,128)(2,1)} %bitcast.31), calls=%async_computation | async-start | bytes 262144 | tf_op jit(solution)/shard_map/all_to_all | solution.py:82
  35.9 132.3 %all-gather.2.cloned.1.call-start = ((), (), s32[]{:S(2)}) async-start(), calls=%async_computation.4 | async-start | bytes 7864320 | tf_op jit(solution)/shard_map/all_gather | solution.py:114
  41.3 1.9 copy-start.6
  177.2 6.3 %copy-start.12 = (bf16[2,2048,256]{2,1,0:T(8,128)(2,1)S(1)}, bf16[2,2048,256]{2,1,0:T(8,128)(2,1)}, u32[]{:S(2)}) copy-start(bf16[2,2048,256]{2,1,0:T(8,128)(2,1)} %param.29) | copy-start | bytes 6291460
  183.5 3.0 copy-start.2
  183.5 3.5 copy-start.14
  194.6 6.3 %copy-start.13 = (bf16[2,2048,256]{2,1,0:T(8,128)(2,1)S(1)}, bf16[2,2048,256]{2,1,0:T(8,128)(2,1)}, u32[]{:S(2)}) copy-start(bf16[2,2048,256]{2,1,0:T(8,128)(2,1)} %param.29) | copy-start | bytes 6291460
  200.9 3.0 copy-start.3
  201.0 3.5 copy-start.15
  204.4 3.8 %copy-start.4 = (bf16[2,256,2048]{2,1,0:T(8,128)(2,1)S(1)}, bf16[2,256,2048]{2,1,0:T(8,128)(2,1)}, u32[]{:S(2)}) copy-start(bf16[2,256,2048]{2,1,0:T(8,128)(2,1)} %param.31) | copy-start | bytes 6291460
  208.2 2.1 copy-start.5
  293.9 12.1 %copy-start.9 = (f32[128,2]{0,1:T(2,128)S(1)}, f32[128,2]{0,1:T(2,128)}, u32[]{:S(2)}) copy-start(f32[128,2]{0,1:T(2,128)} %param.28) | copy-start | bytes 3076
  293.9 12.1 %copy-start.10 = (f32[128]{0:T(128)S(1)}, f32[128]{0:T(128)}, u32[]{:S(2)}) copy-start(f32[128]{0:T(128)} %param.27) | copy-start | bytes 1540
  293.9 51.1 %all-to-all-start.3 = ((bf16[64,2,3,2048]{3,1,2,0:T(2,128)(2,1)}), bf16[64,2,3,2048]{3,1,2,0:T(2,128)(2,1)S(1)}, u32[]{:S(2)}, u32[]{:S(2)}) async-start(bf16[64,2,3,2048]{3,1,2,0:T(2,128)(2,1)} %copy.52), calls=%async_computation.3 | async-start | bytes 3145728 | tf_op jit(solution)/shard_map/all_to_all | solution.py:120
  357.1 5.9 %copy-start.1 = (bf16[512,2048]{1,0:T(8,128)(2,1)S(1)}, bf16[512,2048]{1,0:T(8,128)(2,1)}, u32[]{:S(2)}) copy-start(bf16[512,2048]{1,0:T(8,128)(2,1)} %param.24) | copy-start | bytes 6291460
Sparse Core Ops, SparseCore 0:
  104.9 63.1 all-gather.1
where the time goes:
time: 371 us; the launch traced here: 370 us
  blocking collectives  124 us (33%)
  waiting for transfers between devices  107 us (29%)
  local copies, waits for them, and re-layouts  65.7 us (18%)
  starting transfers between devices  26.1 us (7%)
  other arithmetic  19.2 us (5%)
  between operations  13.8 us (4%)
  matrix products  13.4 us (4%)
    all_to_all x1, blocking collectives, body(): lax.all_to_all(split_quarters(partial_value, tp_count), 'tp', split_axis=...  73.9 us
    all_gather x1, waiting for transfers between devices, body(): arrived = lax.all_gather(arrived_own, 'tp', axis=2, tiled=True)  63.3 us
    all_to_all x1, blocking collectives, body(): lax.all_to_all(outgoing, 'sp', split_axis=0, concat_axis=0, tiled=True)  50.4 us
    all_to_all x1, waiting for transfers between devices, body(): lax.all_to_all(summed, 'sp', split_axis=0, concat_axis=0, tiled=True)  38.9 us
    slice x3, local copies, waits for them, and re-layouts, apply_experts(): rows = arrived[:, local].reshape(-1, arrived.shape[3])  14.7 us
    another operation x2, local copies, waits for them, and re-layouts, apply_experts(): rows = arrived[:, local].reshape(-1, arrived.shape[3])  12.6 us
    all_to_all x1, starting transfers between devices, body(): lax.all_to_all(summed, 'sp', split_axis=0, concat_axis=0, tiled=True)  12.1 us
    ppermute x3, starting transfers between devices, passed_along(): return lax.ppermute(x, axis, pairs)  10.1 us
  transfers between devices with their start and end apart: 6, of which 3 were waited for; matrix products, arithmetic and copies ran while one was open for 3% of the time, Pallas kernels for 0%

commit v1 on v0

--- a/solution.py
+++ b/solution.py
@@ -4,6 +4,13 @@
 from jax.sharding import PartitionSpec as P
 
 eps = 1e-06
+
+
+def exchange_gather(array, axis, along):
+    size = lax.axis_size(axis)
+    blocks = jnp.stack([array for _ in range(size)])
+    blocks = lax.all_to_all(blocks, axis, split_axis=0, concat_axis=0)
+    return jnp.concatenate(blocks, axis=along)
 
 
 def passed_along(x, axis, by):
@@ -111,7 +118,7 @@
     with_blank = jnp.concatenate([normed, jnp.zeros((1, normed.shape[1]), jnp.bfloat16)], axis=0)
     outgoing = with_blank[source].reshape(sp_count, local_experts, capacity, normed.shape[1])
     arrived_own = lax.all_to_all(outgoing, "sp", split_axis=0, concat_axis=0, tiled=True)
-    arrived = lax.all_gather(arrived_own, "tp", axis=2, tiled=True)
+    arrived = exchange_gather(arrived_own, "tp", 2)
     partial_value = apply_experts(arrived, expert_gate, expert_up, expert_down)
     quarters = lax.all_to_all(
         split_quarters(partial_value, tp_count), "tp", split_axis=2, concat_axis=2, tiled=True

time: 371 us -> 362 us (0.976)
  blocking collectives: 124 us -> 195 us
  waiting for transfers between devices: 107 us -> 44 us
  between operations: 13.8 us -> 0.44 us
    all_to_all x0 -> x1, blocking collectives: none -> 72.2 us  [exchange_gather(): blocks = lax.all_to_all(blocks, axis, split_axis=0, concat_axis=0)]
    all_gather x1 -> x0, waiting for transfers between devices: 63.3 us -> none  [body(): arrived = lax.all_gather(arrived_own, 'tp', axis=2, tiled=True)]
  transfers between devices with their start and end apart: 6 -> 5, of which waited for: 3 -> 2; matrix products, arithmetic and copies ran while one was open for 3% -> 3% of each run, Pallas kernels for 0% -> 0%
where the time goes in v1:
time: 362 us; the launch traced here: 361 us
  blocking collectives  195 us (54%)
  local copies, waits for them, and re-layouts  63.4 us (18%)
  waiting for transfers between devices  44 us (12%)
  starting transfers between devices  25 us (7%)
  other arithmetic  19.7 us (5%)
  matrix products  13.4 us (4%)
    all_to_all x1, blocking collectives, body(): lax.all_to_all(split_quarters(partial_value, tp_count), 'tp', split_axis=...  72.3 us
    all_to_all x1, blocking collectives, exchange_gather(): blocks = lax.all_to_all(blocks, axis, split_axis=0, concat_axis=0)  72.2 us
    all_to_all x1, blocking collectives, body(): lax.all_to_all(outgoing, 'sp', split_axis=0, concat_axis=0, tiled=True)  50.4 us
    all_to_all x1, waiting for transfers between devices, body(): lax.all_to_all(summed, 'sp', split_axis=0, concat_axis=0, tiled=True)  38.9 us
    another operation x2, local copies, waits for them, and re-layouts, apply_experts(): rows = arrived[:, local].reshape(-1, arrived.shape[3])  12.6 us
    slice x3, local copies, waits for them, and re-layouts, apply_experts(): rows = arrived[:, local].reshape(-1, arrived.shape[3])  11.6 us
    all_to_all x1, starting transfers between devices, body(): lax.all_to_all(summed, 'sp', split_axis=0, concat_axis=0, tiled=True)  10.8 us
    ppermute x3, starting transfers between devices, passed_along(): return lax.ppermute(x, axis, pairs)  10.1 us
  transfers between devices with their start and end apart: 5, of which 2 were waited for; matrix products, arithmetic and copies ran while one was open for 3% of the time, Pallas kernels for 0%

profile of v1, /device:TPU:1, one launch (start us, length us, event | category | flops | bytes accessed | tf_op | source)
XLA Modules:
  0.0 361.0 jit_solution(17213025763822567921)
XLA Ops:
  0.9 4.6 %collective-permute-start.2 = (s32[30]{0:T(128)S(1)}, s32[30]{0:T(128)S(1)}, u32[]{:S(2)}, u32[]{:S(2)}) collective-permute-start(s32[30]{0:T(128)S(1)} %slice.325), channel_id=1, source_target_pairs={{0,4},{4,8},{8,12},{12,16},{16,20},{20,24},{24,28},{28,32},{32,36}... | collective-permute-start | bytes 368 | tf_op jit(solution)/shard_map/ppermute | solution.py:19
  6.2 1.9 collective-permute-start
  8.8 3.6 collective-permute-start.1
  21.9 4.1 %fusion.25 = bf16[512,128]{1,0:T(8,128)(2,1)} fusion(f32[542,128]{1,0:T(8,128)S(1)} %divide_multiply_fusion, f32[128]{0:T(128)S(1)} %get-tuple-element.38, f32[128]{0:T(128)S(1)} %get-tuple-element.39, f32[128]{0:T(128)S(1)} %get-tuple-element.10, f32[128]{0:T(128)S(1)} %get-tuple-element.11, f32[128]{0:T(128)S(1)} %get-tuple-element.12, ...), kind=kLoop, calls=%fused_computation.43 | loop fusion | flops 6094848 | bytes 8289280 | tf_op jit(solution)/shard_map/convert_element_type | solution.py:34
  26.0 4.1 %all-to-all-start = ((bf16[4,128,128]{2,1,0:T(8,128)(2,1)}), bf16[4,128,128]{2,1,0:T(8,128)(2,1)S(1)}, u32[]{:S(2)}, u32[]{:S(2)}) async-start(bf16[4,128,128]{2,1,0:T(8,128)(2,1)} %bitcast.31), calls=%async_computation | async-start | bytes 262144 | tf_op jit(solution)/shard_map/all_to_all | solution.py:89
  30.1 5.1 %all-to-all-done = bf16[4,128,128]{2,1,0:T(8,128)(2,1)S(1)} async-done(((bf16[4,128,128]{2,1,0:T(8,128)(2,1)}), bf16[4,128,128]{2,1,0:T(8,128)(2,1)S(1)}, u32[]{:S(2)}, u32[]{:S(2)}) %all-to-all-start) | async-done | bytes 131104 | tf_op jit(solution)/shard_map/all_to_all | solution.py:89
  35.7 1.6 multiply_reduce_fusion.1
  37.6 3.1 gather_fusion
  40.7 4.0 %reshape.169 = bf16[64,2,3,2048]{3,2,1,0:T(4,128)(2,1)S(1)} reshape(bf16[384,2048]{1,0:T(8,128)(2,1)} %gather_fusion) | data formatting | bytes 3145728 | tf_op jit(solution)/shard_map/reshape | solution.py:119
  44.7 2.1 copy.50
  46.8 50.4 %all_to_all.33 = bf16[64,2,3,2048]{3,1,2,0:T(2,128)(2,1)S(1)} all-to-all(bf16[64,2,3,2048]{3,1,2,0:T(2,128)(2,1)S(1)} %copy.50), channel_id=1, replica_groups=mesh['sp'=64,'tp'=4] {'sp'}, dimensions={0} | all-to-all | bytes 3145728 | tf_op jit(solution)/shard_map/all_to_all | solution.py:120
  98.7 72.2 %all_to_all.34 = bf16[4,64,2,3,2048]{4,1,3,2,0:T(8,128)(2,1)S(1)} all-to-all(bf16[4,64,2,3,2048]{4,1,3,2,0:T(8,128)(2,1)S(1)} %stack.22), channel_id=1, replica_groups=mesh['sp'=64,'tp'=4] {'tp'}, dimensions={0} | all-to-all | bytes 12582912 | tf_op jit(solution)/shard_map/all_to_all | solution.py:12
  172.0 2.3 fusion.97
  174.3 3.7 %copy.53 = bf16[64,1,12,2048]{3,2,0,1:T(8,128)(2,1)} copy(bf16[64,1,12,2048]{3,0,2,1:T(8,128)(2,1)S(1)} %get-tuple-element.7) | data formatting | bytes 6291456 | tf_op jit(solution)/shard_map/slice | solution.py:46
  178.0 6.3 %reshape_squeeze.6 = bf16[768,2048]{1,0:T(8,128)(2,1)} reshape(bf16[64,1,12,2048]{3,2,0,1:T(8,128)(2,1)} %copy.53) | data formatting | bytes 6291456 | tf_op jit(solution)/shard_map/reshape;squeeze | solution.py:46
  184.3 3.0 fusion.12
  189.7 5.6 %copy.55 = bf16[64,1,12,2048]{3,2,0,1:T(8,128)(2,1)} copy(bf16[64,1,12,2048]{3,0,2,1:T(8,128)(2,1)} %get-tuple-element.8) | data formatting | bytes 6291456 | tf_op jit(solution)/shard_map/slice | solution.py:46
  195.4 6.3 %reshape_squeeze.7 = bf16[768,2048]{1,0:T(8,128)(2,1)} reshape(bf16[64,1,12,2048]{3,2,0,1:T(8,128)(2,1)} %copy.55) | data formatting | bytes 6291456 | tf_op jit(solution)/shard_map/reshape;squeeze | solution.py:46
  201.7 3.0 fusion.9
  205.2 1.7 fusion.5
  206.9 2.1 reshape.173
  209.0 2.1 fusion
  213.8 72.3 %all_to_all.35 = bf16[64,2,4,3,2048]{4,0,3,1,2:T(8,128)(2,1)} all-to-all(bf16[64,2,4,3,2048]{4,0,3,1,2:T(8,128)(2,1)S(1)} %copy.57), channel_id=1, replica_groups=mesh['sp'=64,'tp'=4] {'tp'}, dimensions={2} | all-to-all | bytes 12582912 | tf_op jit(solution)/shard_map/all_to_all | solution.py:123
  286.1 4.2 %reduce_sum.64 = bf16[64,2,3,2048]{3,0,2,1:T(8,128)(2,1)S(1)} reduce(bf16[64,2,4,3,2048]{4,0,3,1,2:T(8,128)(2,1)} %all_to_all.35, bf16[]{:T(256)} %constant.46.clone.1), dimensions={2}, to_apply=%region_7.8 | reduce | flops 2359296 | bytes 7864322 | tf_op jit(solution)/shard_map/reduce_sum | solution.py:126
  290.3 2.8 copy.59
  293.1 10.8 %all-to-all-start.4 = ((bf16[64,2,3,2048]{3,1,2,0:T(2,128)(2,1)}), bf16[64,2,3,2048]{3,1,2,0:T(2,128)(2,1)S(1)}, u32[]{:S(2)}, u32[]{:S(2)}) async-start(bf16[64,2,3,2048]{3,1,2,0:T(2,128)(2,1)} %copy.59), calls=%async_computation.4 | async-start | bytes 3145728 | tf_op jit(solution)/shard_map/all_to_all | solution.py:127
  304.1 38.9 %all-to-all-done.4 = bf16[64,2,3,2048]{3,1,2,0:T(2,128)(2,1)S(1)} async-done(((bf16[64,2,3,2048]{3,1,2,0:T(2,128)(2,1)}), bf16[64,2,3,2048]{3,1,2,0:T(2,128)(2,1)S(1)}, u32[]{:S(2)}, u32[]{:S(2)}) %all-to-all-start.4) | async-done | bytes 1572896 | tf_op jit(solution)/shard_map/all_to_all | solution.py:127
  343.0 2.4 copy.60
  345.4 3.9 %reshape.174 = bf16[384,2048]{1,0:T(8,128)(2,1)S(1)} reshape(bf16[64,2,3,2048]{3,2,1,0:T(4,128)(2,1)} %copy.60) | data formatting | bytes 3145728 | tf_op jit(solution)/shard_map/reshape | solution.py:128
  349.3 2.3 gather_fusion.1
  351.7 3.5 reshape.178
  355.2 4.8 %multiply_reduce_fusion = f32[128,2048]{1,0:T(8,128)S(1)} fusion(f32[128,2,2048]{2,1,0:T(2,128)} %reshape.178, f32[128,2]{1,0:T(8,128)S(1)} %copy.44), kind=kLoop, calls=%fused_computation.11 | loop fusion | flops 786432 | bytes 3146752 | tf_op jit(solution)/shard_map/reduce_sum | solution.py:130
  (83 shorter events, 21.6 us)
Async XLA Ops:
  0.0 35.7 %copy-start = (bf16[512,2048]{1,0:T(8,128)(2,1)S(1)}, bf16[512,2048]{1,0:T(8,128)(2,1)}, u32[]{:S(2)}) copy-start(bf16[512,2048]{1,0:T(8,128)(2,1)} %param.24) | copy-start | bytes 6291460
  0.9 17.5 %collective-permute-start.2 = (s32[30]{0:T(128)S(1)}, s32[30]{0:T(128)S(1)}, u32[]{:S(2)}, u32[]{:S(2)}) collective-permute-start(s32[30]{0:T(128)S(1)} %slice.325), channel_id=1, source_target_pairs={{0,4},{4,8},{8,12},{12,16},{16,20},{20,24},{24,28},{28,32},{32,36}... | collective-permute-start | bytes 368 | tf_op jit(solution)/shard_map/ppermute | solution.py:19
  6.2 14.5 %collective-permute-start = (bf16[30,128]{1,0:T(8,128)(2,1)S(1)}, bf16[30,128]{1,0:T(8,128)(2,1)S(1)}, u32[]{:S(2)}, u32[]{:S(2)}) collective-permute-start(bf16[30,128]{1,0:T(8,128)(2,1)S(1)} %slice.321), channel_id=1, source_target_pairs={{0,4},{4,8},{8,12},{12,16},{16,20},{20,24},{24,28},{28,32},{32,36}... | collective-permute-start | bytes 23048 | tf_op jit(solution)/shard_map/ppermute | solution.py:19
  8.8 11.9 %collective-permute-start.1 = (bf16[30,128]{1,0:T(8,128)(2,1)S(1)}, bf16[30,128]{1,0:T(8,128)(2,1)S(1)}, u32[]{:S(2)}, u32[]{:S(2)}) collective-permute-start(bf16[30,128]{1,0:T(8,128)(2,1)S(1)} %slice.322), channel_id=1, source_target_pairs={{0,4},{4,8},{8,12},{12,16},{16,20},{20,24},{24,28},{28,32},{32,36}... | collective-permute-start | bytes 23048 | tf_op jit(solution)/shard_map/ppermute | solution.py:19
  21.8 13.7 %copy-start.7 = (f32[512]{0:T(512)S(1)}, f32[512]{0:T(512)}, u32[]{:S(2)}) copy-start(f32[512]{0:T(512)} %param.23) | copy-start | bytes 6148
  21.8 13.7 %copy-start.8 = (f32[512]{0:T(512)S(1)}, f32[512]{0:T(512)}, u32[]{:S(2)}) copy-start(f32[512]{0:T(512)} %param.22) | copy-start | bytes 6148
  26.0 11.4 %copy-start.6 = (f32[2048]{0:T(1024)S(1)}, f32[2048]{0:T(1024)}, u32[]{:S(2)}) copy-start(f32[2048]{0:T(1024)} %param.25) | copy-start | bytes 24580
  26.0 9.2 %all-to-all-start = ((bf16[4,128,128]{2,1,0:T(8,128)(2,1)}), bf16[4,128,128]{2,1,0:T(8,128)(2,1)S(1)}, u32[]{:S(2)}, u32[]{:S(2)}) async-start(bf16[4,128,128]{2,1,0:T(8,128)(2,1)} %bitcast.31), calls=%async_computation | async-start | bytes 262144 | tf_op jit(solution)/shard_map/all_to_all | solution.py:89
  178.0 6.3 %copy-start.11 = (bf16[2,2048,256]{2,1,0:T(8,128)(2,1)S(1)}, bf16[2,2048,256]{2,1,0:T(8,128)(2,1)}, u32[]{:S(2)}) copy-start(bf16[2,2048,256]{2,1,0:T(8,128)(2,1)} %param.29) | copy-start | bytes 6291460
  184.3 3.0 copy-start.2
  184.3 3.5 copy-start.13
  195.3 6.3 %copy-start.12 = (bf16[2,2048,256]{2,1,0:T(8,128)(2,1)S(1)}, bf16[2,2048,256]{2,1,0:T(8,128)(2,1)}, u32[]{:S(2)}) copy-start(bf16[2,2048,256]{2,1,0:T(8,128)(2,1)} %param.29) | copy-start | bytes 6291460
  201.7 3.0 copy-start.3
  201.7 3.5 copy-start.14
  205.2 3.8 %copy-start.4 = (bf16[2,256,2048]{2,1,0:T(8,128)(2,1)S(1)}, bf16[2,256,2048]{2,1,0:T(8,128)(2,1)}, u32[]{:S(2)}) copy-start(bf16[2,256,2048]{2,1,0:T(8,128)(2,1)} %param.31) | copy-start | bytes 6291460
  209.0 2.1 copy-start.5
  290.3 13.6 %copy-start.9 = (f32[128,2]{0,1:T(2,128)S(1)}, f32[128,2]{0,1:T(2,128)}, u32[]{:S(2)}) copy-start(f32[128,2]{0,1:T(2,128)} %param.28) | copy-start | bytes 3076
  290.3 13.6 %copy-start.10 = (f32[128]{0:T(128)S(1)}, f32[128]{0:T(128)}, u32[]{:S(2)}) copy-start(f32[128]{0:T(128)} %param.27) | copy-start | bytes 1540
  293.1 49.9 %all-to-all-start.4 = ((bf16[64,2,3,2048]{3,1,2,0:T(2,128)(2,1)}), bf16[64,2,3,2048]{3,1,2,0:T(2,128)(2,1)S(1)}, u32[]{:S(2)}, u32[]{:S(2)}) async-start(bf16[64,2,3,2048]{3,1,2,0:T(2,128)(2,1)} %copy.59), calls=%async_computation.4 | async-start | bytes 3145728 | tf_op jit(solution)/shard_map/all_to_all | solution.py:127
  351.7 9.3 %copy-start.1 = (bf16[512,2048]{1,0:T(8,128)(2,1)S(1)}, bf16[512,2048]{1,0:T(8,128)(2,1)}, u32[]{:S(2)}) copy-start(bf16[512,2048]{1,0:T(8,128)(2,1)} %param.24) | copy-start | bytes 6291460
